TPU v7x, 512 devices: a whole 4x8x8 slice. The times are simulated.
512 devices in a mesh: row: 64 (over z, y), col: 8 (over x, core).
Axes of the slice: x: 4, y: 8, z: 8, core: 2. Of those that a mesh axis runs over, the one named last changes fastest.
Arguments:
- tokens: bfloat16 [8, 24576, 2048], P('col', 'row'), may hold values from -6 to 6
- norm_gain: bfloat16 [2048], replicated, may hold values from 0.099609375 to 1.8984375
- in_weight: bfloat16 [2048, 512], P('row', 'col'), may hold values from -0.125 to 0.125
- out_weight: bfloat16 [512, 2048], P('col', 'row'), may hold values from -0.25 to 0.25
Outputs:
- mixed: bfloat16 [8, 24576, 2048], P('col', 'row')
All inputs are finite; a program needn't handle non-finite values.
Results may differ from a plain program's by a relative error of at most 0.013.
Values may be sent and summed in bfloat16 or wider, within the bound.
A program may use at most 64 MiB of HBM per device.

v0:
```python
import math

import jax
import jax.numpy as jnp
from jax import lax
from jax.sharding import Mesh
from jax.sharding import PartitionSpec as P

GS = 64
ROW = ("row_0", "row_1")


EPS = 1e-06


def turned_gather(arrays, axis, dims):
    turned = [jnp.moveaxis(a, dim, 0) for a, dim in zip(arrays, dims)]
    widths = [t[0].size for t in turned]
    both = jnp.concatenate([t.reshape(-1, w) for t, w in zip(turned, widths)], axis=1)
    out = lax.all_gather(both, axis, axis=0, tiled=True)
    pieces = jnp.split(out, [sum(widths[:k]) for k in range(1, len(widths))], axis=1)
    return tuple(
        (
            jnp.moveaxis(b.reshape(-1, *t.shape[1:]), 0, dim)
            for b, t, dim in zip(pieces, turned, dims)
        )
    )


def joined_along(pieces, dim):
    pieces = jnp.moveaxis(pieces, 0, dim)
    lengths = pieces.shape
    return pieces.reshape(*lengths[:dim], lengths[dim] * lengths[dim + 1], *lengths[dim + 2 :])


def all_blocks(shard, axes, sequence):
    pieces = shard
    for k in sequence:
        pieces = lax.all_gather(pieces, axes[k])
    done = sequence[::-1]
    back = [done.index(k) for k in range(len(axes))]
    pieces = pieces.transpose(*back, *range(len(axes), pieces.ndim))
    return pieces.reshape(-1, *shard.shape)


def gather_axes(shard, axes, sequence, dim):
    return joined_along(all_blocks(shard, axes, sequence), dim)


def angle_pair(left_index, right_index, modulus):
    product = left_index[:, None] * right_index[None, :] % modulus
    radians = product.astype(jnp.float32) * (2.0 * math.pi / modulus)
    return (jnp.cos(radians), jnp.sin(radians))


def table_dot(matrix, values):
    return jnp.dot(matrix, values, preferred_element_type=jnp.float32)


def right_dot(values, matrix):
    return jnp.dot(values, matrix, preferred_element_type=jnp.float32)


def body(tokens, norm_gain, in_weight, out_weight):
    own_rows = tokens[0].astype(jnp.float32)
    inverse_rms = lax.rsqrt(jnp.mean(own_rows * own_rows, axis=-1, keepdims=True) + EPS)
    normed = (own_rows * inverse_rms * norm_gain.astype(jnp.float32)).astype(jnp.bfloat16)
    in_columns, out_rows = turned_gather((in_weight, out_weight), "col", (1, 0))
    row_count = normed.shape[0]
    channels = in_columns.shape[1]
    peer_count = lax.axis_size(ROW)
    length = row_count * peer_count
    projected = jnp.dot(
        normed, gather_axes(in_columns, ROW, (0, 1), 0), preferred_element_type=jnp.float32
    ).astype(jnp.bfloat16)
    channel_index = jnp.arange(channels, dtype=jnp.int32)
    within = channel_index % GS
    same_group = channel_index[:, None] // GS == channel_index[None, :] // GS
    group_cos, group_sin = angle_pair(within, within, GS)
    group_cos = jnp.where(same_group, group_cos, 0.0)
    group_sin = jnp.where(same_group, group_sin, 0.0)
    peer_index = jnp.arange(peer_count, dtype=jnp.int32)
    small_cos, small_sin = angle_pair(peer_index, peer_index, peer_count)
    line_index = jnp.arange(row_count, dtype=jnp.int32)
    long_cos, long_sin = angle_pair(line_index, line_index, row_count)
    gathered = lax.all_to_all(projected, ROW, split_axis=1, concat_axis=0, tiled=True).astype(
        jnp.float32
    )
    narrow = gathered.shape[1]
    flat = gathered.reshape(peer_count, row_count * narrow)
    first_real = table_dot(small_cos, flat).reshape(peer_count, row_count, narrow)
    first_imag = (-table_dot(small_sin, flat)).reshape(peer_count, row_count, narrow)
    turn_cos, turn_sin = angle_pair(peer_index, line_index, length)
    turn_cos = turn_cos[:, :, None]
    turn_sin = turn_sin[:, :, None]
    turned_real = first_real * turn_cos + first_imag * turn_sin
    turned_imag = first_imag * turn_cos - first_real * turn_sin
    lines_real = turned_real.transpose(1, 0, 2).reshape(row_count, peer_count * narrow)
    lines_imag = turned_imag.transpose(1, 0, 2).reshape(row_count, peer_count * narrow)
    whole_real = (table_dot(long_cos, lines_real) + table_dot(long_sin, lines_imag)).reshape(
        length, narrow
    )
    whole_imag = (table_dot(long_cos, lines_imag) - table_dot(long_sin, lines_real)).reshape(
        length, narrow
    )
    back_real, back_imag = (
        lax.all_to_all(
            whole_real.astype(jnp.bfloat16), ROW, split_axis=0, concat_axis=1, tiled=True
        ).astype(whole_real.dtype),
        lax.all_to_all(
            whole_imag.astype(jnp.bfloat16), ROW, split_axis=0, concat_axis=1, tiled=True
        ).astype(whole_imag.dtype),
    )
    mixed_real = right_dot(back_real, group_cos) + right_dot(back_imag, group_sin)
    arranged = (mixed_real * (1.0 / math.sqrt(length * GS))).astype(jnp.bfloat16)
    result = jnp.dot(
        arranged,
        lax.all_gather(out_rows, ROW, axis=1, tiled=True),
        preferred_element_type=jnp.float32,
    )
    return result.astype(jnp.bfloat16)[None]


def solution(mesh):
    split = Mesh(mesh.devices.reshape(8, 8, mesh.shape["col"]), ("row_0", "row_1", "col"))
    in_specs = (P("col", ROW, None), P(), P(ROW, "col"), P("col", ROW))
    out_specs = P("col", ROW, None)
    return jax.shard_map(body, mesh=split, in_specs=in_specs, out_specs=out_specs, check_vma=False)
```

profile of v0, /device:TPU:4, one launch (start us, length us, event | category | flops | bytes accessed | tf_op | source)
XLA Modules:
  0.0 213.6 jit_solution(14317200805764714633)
XLA Ops:
  6.5 0.0 copy-start
  6.5 0.0 all-gather.7.cloned.1.call-start
  6.5 0.9 copy.54
  7.4 0.8 copy.55
  8.2 0.1 pad_maximum_fusion
  8.3 16.5 %all_gather.18 = bf16[512,64]{1,0:T(8,128)(2,1)S(1)} all-gather(bf16[64,64]{1,0:T(8,128)(2,1)S(1)} %pad_maximum_fusion), channel_id=1, replica_groups=mesh['row_0'=8,'row_1'=8,'col'=8] {'col'}, dimensions={0}, use_global_device_ids=true | all-gather | bytes 73728 | tf_op jit(solution)/shard_map/all_gather | solution.py:20
  24.8 0.1 fusion.135
  25.0 0.1 copy.70
  25.0 28.2 %all-gather = bf16[256,512]{1,0:T(8,128)(2,1)} all-gather(bf16[32,512]{1,0:T(8,128)(2,1)S(1)} %bitcast.62), channel_id=2, replica_groups=mesh['row_0'=8,'row_1'=8,'col'=8] {'row_0'}, dimensions={0}, use_global_device_ids=true | all-gather | bytes 294912 | tf_op jit(solution)/shard_map/all_gather | solution.py:39
  53.2 0.0 all-gather.7.cloned.1.call-update
  53.2 0.0 all-gather.5.cloned.1.call-start
  53.3 0.7 copy.68
  54.0 0.0 all-gather.5.cloned.1.call-update
  54.0 0.7 convert_element_type.78
  54.7 0.0 copy-done
  54.7 0.4 fusion
  55.1 40.9 %all-gather.7.cloned.1.call-done = bf16[64,32,512]{2,1,0:T(8,128)(2,1)} async-done(((bf16[8,32,512]{2,1,0:T(8,128)(2,1)}), bf16[64,32,512]{2,1,0:T(8,128)(2,1)}) %all-gather.7.cloned.1.call-update) | async-done | bytes 2097168 | tf_op jit(solution)/shard_map/all_gather | solution.py:39
  96.0 1.8 copy.57
  97.9 1.0 fusion.13
  98.9 0.9 copy.58
  99.8 10.7 %all-to-all-start = ((bf16[384,64,8]{0,2,1:T(8,128)(2,1)}), bf16[384,64,8]{0,2,1:T(8,128)(2,1)S(1)}, u32[]{:S(2)}, u32[]{:S(2)}) async-start(bf16[384,64,8]{0,2,1:T(8,128)(2,1)} %bitcast.8), calls=%async_computation | async-start | bytes 786432 | tf_op jit(solution)/shard_map/all_to_all | solution.py:86
  110.5 0.4 fusion.78
  111.0 14.1 %all-to-all-done = bf16[384,64,8]{0,2,1:T(8,128)(2,1)S(1)} async-done(((bf16[384,64,8]{0,2,1:T(8,128)(2,1)}), bf16[384,64,8]{0,2,1:T(8,128)(2,1)S(1)}, u32[]{:S(2)}, u32[]{:S(2)}) %all-to-all-start) | async-done | bytes 393248 | tf_op jit(solution)/shard_map/all_to_all | solution.py:86
  125.1 0.6 copy.59
  125.7 0.5 convolution_negate_fusion
  126.2 0.5 copy.61
  126.7 0.5 copy.62
  127.2 0.5 subtract_bitcast_fusion
  127.7 2.5 %fusion.26 = f32[384,512]{1,0:T(8,128)S(1)} fusion(bf16[384,64,8]{0,1,2:T(8,128)(2,1)S(1)} %get-tuple-element.6), kind=kOutput, calls=%fused_computation.38 | convolution fusion | flops 152322048 | bytes 1179648 | tf_op jit(solution)/shard_map/dot_general | solution.py:57
  130.2 2.9 %fusion.10 = bf16[384,512]{1,0:T(8,128)(2,1)S(1)} fusion(f32[384,512]{1,0:T(8,128)S(1)} %fusion.26, bf16[384,64,8]{0,1,2:T(8,128)(2,1)S(1)} %get-tuple-element.5), kind=kOutput, calls=%fused_computation.23 | convolution fusion | flops 152715264 | bytes 1572864 | tf_op jit(solution)/shard_map/dot_general | solution.py:57
  133.1 8.4 %convert_element_type.84 = bf16[64,384,8]{2,1,0:T(8,128)(2,1)} reshape(bf16[384,512]{1,0:T(8,128)(2,1)S(1)} %fusion.10) | data formatting | bytes 786432 | tf_op jit(solution)/shard_map/convert_element_type | solution.py:108
  141.5 5.8 %copy.66 = bf16[64,384,8]{1,2,0:T(8,128)(2,1)} copy(bf16[64,384,8]{2,1,0:T(8,128)(2,1)} %convert_element_type.84) | data formatting | bytes 786432 | tf_op jit(solution)/shard_map/convert_element_type | solution.py:108
  147.3 4.8 %all-to-all-start.1 = ((bf16[64,384,8]{1,2,0:T(8,128)(2,1)}), bf16[64,384,8]{1,2,0:T(8,128)(2,1)S(1)}, u32[]{:S(2)}, u32[]{:S(2)}) async-start(bf16[64,384,8]{1,2,0:T(8,128)(2,1)} %copy.66), calls=%async_computation.1 | async-start | bytes 786432 | tf_op jit(solution)/shard_map/all_to_all | solution.py:107
  152.1 2.5 %fusion.22 = f32[384,512]{1,0:T(8,128)S(1)} fusion(bf16[384,64,8]{0,1,2:T(8,128)(2,1)S(1)} %get-tuple-element.5), kind=kOutput, calls=%fused_computation.34 | convolution fusion | flops 152322048 | bytes 1179648 | tf_op jit(solution)/shard_map/dot_general | solution.py:57
  154.6 2.9 %fusion.11 = bf16[384,512]{1,0:T(8,128)(2,1)S(1)} fusion(f32[384,512]{1,0:T(8,128)S(1)} %fusion.22, bf16[384,64,8]{0,1,2:T(8,128)(2,1)S(1)} %get-tuple-element.6), kind=kOutput, calls=%fused_computation.24 | convolution fusion | flops 152715264 | bytes 1572864 | tf_op jit(solution)/shard_map/dot_general | solution.py:57
  157.5 8.4 %convert_element_type.87 = bf16[64,384,8]{2,1,0:T(8,128)(2,1)} reshape(bf16[384,512]{1,0:T(8,128)(2,1)S(1)} %fusion.11) | data formatting | bytes 786432 | tf_op jit(solution)/shard_map/convert_element_type | solution.py:111
  165.9 5.8 %copy.67 = bf16[64,384,8]{1,2,0:T(8,128)(2,1)} copy(bf16[64,384,8]{2,1,0:T(8,128)(2,1)} %convert_element_type.87) | data formatting | bytes 786432 | tf_op jit(solution)/shard_map/convert_element_type | solution.py:111
  171.7 0.0 all-to-all-done.1
  171.7 12.9 %all-to-all-start.2 = ((bf16[64,384,8]{1,2,0:T(8,128)(2,1)}), bf16[64,384,8]{1,2,0:T(8,128)(2,1)S(1)}, u32[]{:S(2)}, u32[]{:S(2)}) async-start(bf16[64,384,8]{1,2,0:T(8,128)(2,1)} %copy.67), calls=%async_computation.2 | async-start | bytes 786432 | tf_op jit(solution)/shard_map/all_to_all | solution.py:110
  184.7 4.2 %fusion.16 = f32[384,512]{1,0:T(8,128)S(1)} fusion(s32[512]{0:T(512)S(1)} %get-tuple-element.11, s32[512]{0:T(512)S(1)} %get-tuple-element.12, bf16[64,384,8]{1,2,0:T(8,128)(2,1)S(1)} %all-to-all-done.1), kind=kOutput, calls=%fused_computation.27 | convolution fusion | flops 205520896 | bytes 1183744 | tf_op jit(solution)/shard_map/dot_general | solution.py:61
  188.8 0.0 all-gather.5.cloned.1.call-done
  188.9 10.1 %all-to-all-done.2 = bf16[64,384,8]{1,2,0:T(8,128)(2,1)S(1)} async-done(((bf16[64,384,8]{1,2,0:T(8,128)(2,1)}), bf16[64,384,8]{1,2,0:T(8,128)(2,1)S(1)}, u32[]{:S(2)}, u32[]{:S(2)}) %all-to-all-start.2) | async-done | bytes 393248 | tf_op jit(solution)/shard_map/all_to_all | solution.py:110
  199.0 7.8 %fusion.3 = bf16[1,384,2048]{2,1,0:T(8,128)(2,1)} fusion(bf16[512,2048]{0,1:T(8,128)(2,1)} %all-gather.5.cloned.1.call-done, f32[384,512]{1,0:T(8,128)S(1)} %fusion.16, s32[512]{0:T(512)S(1)} %get-tuple-element.11, s32[512]{0:T(512)S(1)} %get-tuple-element.12, bf16[64,384,8]{1,2,0:T(8,128)(2,1)S(1)} %all-to-all-done.2), kind=kOutput, calls=%fused_computation.7 | convolution fusion | flops 1012203520 | bytes 4853760 | tf_op jit(solution)/shard_map/dot_general | solution.py:116
  (2 shorter events, 0.0 us)
Async XLA Ops:
  6.5 48.2 %copy-start = (bf16[1,384,2048]{2,1,0:T(8,128)(2,1)S(1)}, bf16[1,384,2048]{2,1,0:T(8,128)(2,1)}, u32[]{:S(2)}) copy-start(bf16[1,384,2048]{2,1,0:T(8,128)(2,1)} %param.4) | copy-start | bytes 4718596
  6.5 89.5 %all-gather.7.cloned.1.call-start = ((), (), s32[]{:S(2)}) async-start(), calls=%async_computation.4 | async-start | bytes 2359296 | tf_op jit(solution)/shard_map/all_gather | solution.py:39
  53.2 135.6 %all-gather.5.cloned.1.call-start = ((), (), s32[]{:S(2)}) async-start(), calls=%async_computation.3 | async-start | bytes 2129920 | tf_op jit(solution)/shard_map/all_gather | solution.py:118
  99.8 25.3 %all-to-all-start = ((bf16[384,64,8]{0,2,1:T(8,128)(2,1)}), bf16[384,64,8]{0,2,1:T(8,128)(2,1)S(1)}, u32[]{:S(2)}, u32[]{:S(2)}) async-start(bf16[384,64,8]{0,2,1:T(8,128)(2,1)} %bitcast.8), calls=%async_computation | async-start | bytes 786432 | tf_op jit(solution)/shard_map/all_to_all | solution.py:86
  147.3 24.4 %all-to-all-start.1 = ((bf16[64,384,8]{1,2,0:T(8,128)(2,1)}), bf16[64,384,8]{1,2,0:T(8,128)(2,1)S(1)}, u32[]{:S(2)}, u32[]{:S(2)}) async-start(bf16[64,384,8]{1,2,0:T(8,128)(2,1)} %copy.66), calls=%async_computation.1 | async-start | bytes 786432 | tf_op jit(solution)/shard_map/all_to_all | solution.py:107
  171.7 27.3 %all-to-all-start.2 = ((bf16[64,384,8]{1,2,0:T(8,128)(2,1)}), bf16[64,384,8]{1,2,0:T(8,128)(2,1)S(1)}, u32[]{:S(2)}, u32[]{:S(2)}) async-start(bf16[64,384,8]{1,2,0:T(8,128)(2,1)} %copy.67), calls=%async_computation.2 | async-start | bytes 786432 | tf_op jit(solution)/shard_map/all_to_all | solution.py:110
Sparse Core Ops, SparseCore 0:
  53.3 42.6 all-gather.6
  99.1 85.8 all-gather.4
where the time goes:
time: 214 us
  waiting for transfers between devices  65.3 us (31%)
  blocking collectives  44.7 us (21%)
  local copies, waits for them, and re-layouts  35.3 us (16%)
  starting transfers between devices  28.5 us (13%)
  matrix products  24.7 us (12%)
  between operations  13.5 us (6%)
    all_gather x1, waiting for transfers between devices, all_blocks(): pieces = lax.all_gather(pieces, axes[k])  40.9 us
    all_gather x1, blocking collectives, all_blocks(): pieces = lax.all_gather(pieces, axes[k])  28.2 us
    all_gather x1, blocking collectives, turned_gather(): out = lax.all_gather(both, axis, axis=0, tiled=True)  16.5 us
    convert_element_type x2, local copies, waits for them, and re-layouts, body(): whole_imag.astype(jnp.bfloat16)  14.2 us
    convert_element_type x2, local copies, waits for them, and re-layouts, body(): whole_real.astype(jnp.bfloat16)  14.2 us
    all_to_all x1, waiting for transfers between devices, body(): lax.all_to_all(projected, ROW, split_axis=1, concat_axis=0, tiled=True)  14.1 us
    all_to_all x1, starting transfers between devices, body(): lax.all_to_all(whole_imag.astype(jnp.bfloat16), ROW, split_axis=0, concat...  12.9 us
    dot_general x6, matrix products, table_dot(): return jnp.dot(matrix, values, preferred_element_type=jnp.float32)  11.7 us
  transfers between devices with their start and end apart: 5, of which 3 were waited for; matrix products, arithmetic and copies ran while one was open for 24% of the time, Pallas kernels for 0%

commit v1 on v0

v1 whole, which is shorter than its diff:
```python
import functools
import math

import jax
import jax.numpy as jnp
import numpy as np
from jax import lax
from jax.experimental import pallas as pl
from jax.experimental.pallas import tpu as pltpu
from jax.sharding import PartitionSpec as P

GS = 64
HALF = GS // 2
EPS = 1e-06
F32 = jnp.float32
BF16 = jnp.bfloat16
MESH = pl.DeviceIdType.MESH


class Sizes:
    def __init__(self, rows, cols, local, width):
        self.rows = rows
        self.nz = 1 << ((rows.bit_length() - 1 + 1) // 2)
        self.ny = rows // self.nz
        self.nx = cols // 2
        self.local = local
        self.width = width
        self.ch = GS * self.nx
        self.per = 2 * self.ch // rows
        self.pairs = self.per // 2
        self.hops = local // rows
        self.blk = width // rows
        self.tiles = max(1, local // 128)
        self.lane = local // self.tiles


def tables(z):
    rows, local, ch = z.rows, z.local, z.ch
    length = rows * local
    k = np.arange(GS)
    small = np.zeros((GS, GS))
    for j in range(HALF):
        if j == 0:
            small[0] = (1.0 + (-1.0) ** k) / 2
            small[1] = (1.0 - (-1.0) ** k) / 2
        else:
            small[2 * j] = np.cos(2 * math.pi * j * k / GS)
            small[2 * j + 1] = np.sin(2 * math.pi * j * k / GS)
    chan = np.kron(np.eye(z.nx), small)
    i = np.arange(rows)
    ang = 2 * math.pi * np.outer(i, i) / rows
    c, s = np.cos(ang), np.sin(ang)
    first = np.stack(
        [
            np.block([[c, -s], [-s, -c], [c, s], [-s, c]]),
            np.block([[c, c], [-s, -s], [c, -c], [-s, s]]),
        ]
    )
    m = np.arange(local)
    tw = 2 * math.pi * np.outer(i, m) / length
    turn = np.stack([np.cos(tw), np.sin(tw)])
    a = np.arange(z.hops)
    k2 = (z.hops * i[None, :] + a[:, None]).reshape(-1)
    ang2 = 2 * math.pi * (np.outer(k2, m) % local) / local
    scale = 1.0 / math.sqrt(length * GS)
    second = np.concatenate([np.cos(ang2), np.sin(ang2)], axis=1) * scale
    place_in = np.zeros((z.nx, 2 * GS, ch))
    place_out = np.zeros((z.nx, 2 * GS, ch))
    for x in range(z.nx):
        for q in range(GS):
            place_in[x, q, GS * x + q] = 1
        for j in range(HALF):
            place_out[x, GS + j, GS * x + 2 * j] = 1
            other = HALF if j == 0 else GS - j
            place_out[x, GS + other, GS * x + 2 * j + 1] = 1
    bf = lambda t: jnp.asarray(t.astype(np.float32)).astype(BF16)
    return (
        bf(chan),
        bf(first),
        jnp.asarray(turn.astype(np.float32)),
        bf(second),
        bf(place_in),
        bf(place_out),
    )


def dot(a, b):
    return jnp.dot(a, b, preferred_element_type=F32)


def dot_nt(a, b):
    return lax.dot_general(a, b, (((1,), (1,)), ((), ())), preferred_element_type=F32)


def kernel(
    z,
    tok_hbm, gain_ref, blk_ref, chan_hbm, first_hbm, turn_hbm, second_hbm, pin_hbm, pout_hbm,
    out_hbm,
    tok, chan, first, turn, second, pin, pout,
    xbuf, win, wo, ht, got, stage, gp, back, got2, obuf,
    tab_sem, tok_sem, swap_send, swap_recv,
    x_send, x_recv, in_send, in_recv, wo_send, wo_recv, half_send, half_recv,
    a_send, a_recv, b_send, b_recv, o_sem,
):
    rows, ny, nz, nx, local = z.rows, z.ny, z.nz, z.nx, z.local
    r = lax.axis_index("row")
    c = lax.axis_index("col")
    h = lax.rem(c, 2)
    x = c // 2
    zz = r // ny
    yy = lax.rem(r, ny)
    other = c + 1 - 2 * h

    def send(src, dst, ssem, rsem, row, col):
        copy = pltpu.make_async_remote_copy(
            src_ref=src, dst_ref=dst, send_sem=ssem, recv_sem=rsem,
            device_id=(row, col), device_id_type=MESH,
        )
        copy.start()

    def drain(ref, sem):
        pltpu.make_async_copy(ref, ref, sem).wait()

    barrier = pltpu.get_barrier_semaphore()

    def greet(i, carry):
        peer = lax.rem(r + i, rows)
        pl.semaphore_signal(barrier, inc=1, device_id=(peer, c), device_id_type=MESH)
        pl.semaphore_signal(barrier, inc=1, device_id=(peer, other), device_id_type=MESH)
        return carry

    for d in range(1, nx):
        px = lax.rem(x + d, nx)
        pl.semaphore_signal(barrier, inc=1, device_id=(r, 2 * px + h), device_id_type=MESH)
    pl.semaphore_signal(barrier, inc=1, device_id=(r, other), device_id_type=MESH)
    lax.fori_loop(1, rows, greet, 0)

    own = pltpu.make_async_copy(tok_hbm, tok.at[h], tok_sem)
    own.start()
    loads = [
        pltpu.make_async_copy(src, dst, tab_sem.at[n])
        for n, (src, dst) in enumerate(
            [(pin_hbm, pin), (pout_hbm, pout), (chan_hbm, chan), (first_hbm, first),
             (turn_hbm, turn), (second_hbm, second)]
        )
    ]
    for load in loads:
        load.start()
    pl.semaphore_wait(barrier, 2 * rows - 1 + nx - 1)

    for d in range(1, nx):
        px = lax.rem(x + d, nx)
        send(blk_ref, xbuf.at[x], x_send, x_recv, r, 2 * px + h)
    send(tok_hbm, tok.at[h], swap_send, swap_recv, r, other)
    xbuf[x] = blk_ref[...]
    loads[0].wait()
    loads[1].wait()
    drain(xbuf.at[pl.ds(0, nx - 1)], x_recv)

    def assemble(place):
        total = dot(xbuf[0], place[0])
        for n in range(1, nx):
            total += dot(xbuf[n], place[n])
        return total.astype(BF16)

    win[zz, yy] = assemble(pin)
    wo[h, zz, yy] = assemble(pout)

    hb = z.blk // 2
    lo, hi = pl.ds(0, hb), pl.ds(hb, hb)
    wh = wo.at[h]
    for buf, ssem, rsem in ((win, in_send, in_recv), (wh, wo_send, wo_recv)):
        for d in range(1, ny):
            py = lax.rem(yy + d, ny)
            send(buf.at[zz, yy, lo], buf.at[zz, yy, lo], ssem.at[0], rsem.at[0], zz * ny + py, c)
        for d in range(1, nz):
            pz = lax.rem(zz + d, nz)
            send(buf.at[zz, yy, hi], buf.at[zz, yy, hi], ssem.at[1], rsem.at[1], pz * ny + yy, c)

    gain = gain_ref[...].astype(F32)
    step = min(32, local)

    def norm(q):
        def one(i, carry):
            part = pl.ds(pl.multiple_of(i * step, step), step)
            v = tok[q, part, :].astype(F32)
            inv = lax.rsqrt(jnp.mean(v * v, axis=-1, keepdims=True) + EPS)
            tok[q, part, :] = (v * inv * gain).astype(BF16)
            return carry

        lax.fori_loop(0, local // step, one, 0)

    for buf, ssem, rsem in ((win, in_send, in_recv), (wh, wo_send, wo_recv)):
        drain(buf.at[0, pl.ds(0, ny - 1), lo], rsem.at[0])
        drain(buf.at[pl.ds(0, nz - 1), 0, hi], rsem.at[1])
        for d in range(1, nz):
            pz = lax.rem(zz + d, nz)
            send(buf.at[zz, :, lo], buf.at[zz, :, lo], ssem.at[2], rsem.at[2], pz * ny + yy, c)
        for d in range(1, ny):
            py = lax.rem(yy + d, ny)
            send(buf.at[:, yy, hi], buf.at[:, yy, hi], ssem.at[3], rsem.at[3], zz * ny + py, c)

    own.wait()
    norm(h)
    drain(tok.at[0], swap_recv)
    norm(1 - h)
    drain(win.at[pl.ds(0, nz - 1), :, lo], in_recv.at[2])
    drain(win.at[:, pl.ds(0, ny - 1), hi], in_recv.at[3])
    loads[2].wait()

    groups = rows // 2
    weight = win[...].reshape(z.width, z.ch)
    for q in range(2):
        proj = dot(tok[q], weight).astype(BF16)
        cols = dot_nt(chan[...], proj).astype(BF16)
        ht[pl.ds(groups * q, groups)] = cols.reshape(groups, z.per, local)

    def scatter(i, carry):
        peer = lax.rem(r + i, rows)
        send(ht.at[peer], got.at[r], a_send, a_recv, peer, c)
        return carry

    lax.fori_loop(1, rows, scatter, 0)
    got[r] = ht[r]
    for load in loads[3:]:
        load.wait()

    drain(wh.at[pl.ds(0, nz - 1), :, lo], wo_recv.at[2])
    drain(wh.at[:, pl.ds(0, ny - 1), hi], wo_recv.at[3])
    send(wh, wh, half_send, half_recv, r, other)

    drain(got.at[pl.ds(0, rows - 1)], a_recv)

    lane = z.lane
    for l in range(z.tiles):
        part = got[:, :, l * lane:(l + 1) * lane].astype(F32)
        stage[l] = part.reshape(rows * z.per, lane)
    odd = lax.rem(lax.rem(r, groups) * z.pairs, HALF)
    tc, ts = turn[0], turn[1]
    for p in range(z.pairs):
        if p == 0:
            matrix = jnp.where(odd == 0, first[1].astype(F32), first[0].astype(F32)).astype(BF16)
        else:
            matrix = first[0]
        for l in range(z.tiles):
            lanes = slice(l * lane, (l + 1) * lane)
            cos, sin = tc[:, lanes], ts[:, lanes]
            u = stage[l, pl.ds(2 * p, rows, stride=z.per), :]
            v = stage[l, pl.ds(2 * p + 1, rows, stride=z.per), :]
            g = dot(matrix, jnp.concatenate([u, v], axis=0).astype(BF16))
            for w in range(2):
                re = g[2 * w * rows:(2 * w + 1) * rows]
                im = g[(2 * w + 1) * rows:(2 * w + 2) * rows]
                at = pl.ds((2 * p + w) * rows, rows)
                gp[at, l * lane:(l + 1) * lane] = (re * cos + im * sin).astype(BF16)
                gp[at, local + l * lane:local + (l + 1) * lane] = (im * cos - re * sin).astype(BF16)
    spec = dot_nt(second[...], gp[...])
    if rows == GS and lane == 128:
        left = lax.broadcasted_iota(jnp.int32, (rows, lane), 1) < rows
        for l in range(z.tiles):
            for p in range(z.pairs):
                t0 = spec[2 * l * rows:(2 * l + 1) * rows, p * lane:(p + 1) * lane]
                t1 = spec[(2 * l + 1) * rows:(2 * l + 2) * rows, p * lane:(p + 1) * lane]
                stage[l, pl.ds(2 * p, rows, stride=z.per), :] = jnp.where(
                    left, t0, pltpu.roll(t1, rows, 1)
                )
                stage[l, pl.ds(2 * p + 1, rows, stride=z.per), :] = jnp.where(
                    left, pltpu.roll(t0, rows, 1), t1
                )
    else:
        full = spec.reshape(z.hops, rows, z.per, rows).transpose(1, 2, 0, 3)
        full = full.reshape(rows * z.per, z.tiles, lane)
        for l in range(z.tiles):
            stage[l] = full[:, l]
    for l in range(z.tiles):
        back[:, :, l * lane:(l + 1) * lane] = stage[l].reshape(rows, z.per, lane).astype(BF16)

    seq = r // groups
    slot = h * groups + lax.rem(r, groups)
    target = 2 * x + seq

    def give(i, carry):
        peer = lax.rem(r + i, rows)
        send(back.at[peer], got2.at[slot], b_send, b_recv, peer, target)
        return carry

    lax.fori_loop(1, rows, give, 0)

    @pl.when(seq == h)
    def _():
        got2[slot] = back[r]

    @pl.when(seq != h)
    def _():
        send(back.at[r], got2.at[slot], b_send, b_recv, r, target)

    drain(wo.at[0], half_recv)

    @pl.when(seq == h)
    def _():
        drain(got2.at[pl.ds(0, rows - 1)], b_recv)

    @pl.when(seq != h)
    def _():
        drain(got2, b_recv)

    mixed = got2[...].astype(F32).reshape(rows * z.per, local).T.astype(BF16)
    ma, mb = mixed[:, :z.ch], mixed[:, z.ch:]
    chunk = ny * z.blk
    for n in range(nz):
        res = dot_nt(ma, wo[0, n].reshape(chunk, z.ch)) + dot_nt(mb, wo[1, n].reshape(chunk, z.ch))
        obuf[n] = res.astype(BF16)
        pltpu.make_async_copy(obuf.at[n], out_hbm.at[:, pl.ds(n * chunk, chunk)], o_sem.at[n]).start()
    for n in range(nz):
        pltpu.make_async_copy(obuf.at[n], out_hbm.at[:, pl.ds(n * chunk, chunk)], o_sem.at[n]).wait()

    drain(xbuf.at[pl.ds(0, nx - 1)], x_send)
    drain(tok.at[0], swap_send)
    for buf, ssem in ((win, in_send), (wh, wo_send)):
        drain(buf.at[0, pl.ds(0, ny - 1), lo], ssem.at[0])
        drain(buf.at[pl.ds(0, nz - 1), 0, hi], ssem.at[1])
        drain(buf.at[pl.ds(0, nz - 1), :, lo], ssem.at[2])
        drain(buf.at[:, pl.ds(0, ny - 1), hi], ssem.at[3])
    drain(wo.at[0], half_send)
    drain(ht.at[pl.ds(0, rows - 1)], a_send)

    @pl.when(seq == h)
    def _():
        drain(back.at[pl.ds(0, rows - 1)], b_send)

    @pl.when(seq != h)
    def _():
        drain(back, b_send)


def body(rows, cols, tokens, norm_gain, in_weight, out_weight):
    local, width = tokens.shape[1:]
    z = Sizes(rows, cols, local, width)
    block = jnp.concatenate([in_weight, out_weight.T], axis=1)
    consts = tables(z)
    any_spec = pl.BlockSpec(memory_space=pl.ANY)
    vmem = pl.BlockSpec(memory_space=pltpu.VMEM)
    scratch = [pltpu.VMEM((2, local, width), BF16)]
    scratch += [pltpu.VMEM(t.shape, t.dtype) for t in (consts[0], consts[1], consts[2], consts[3], consts[4], consts[5])]
    scratch += [
        pltpu.VMEM((z.nx, z.blk, 2 * GS), BF16),
        pltpu.VMEM((z.nz, z.ny, z.blk, z.ch), BF16),
        pltpu.VMEM((2, z.nz, z.ny, z.blk, z.ch), BF16),
        pltpu.VMEM((rows, z.per, local), BF16),
        pltpu.VMEM((rows, z.per, local), BF16),
        pltpu.VMEM((z.tiles, rows * z.per, z.lane), F32),
        pltpu.VMEM((z.per * rows, 2 * local), BF16),
        pltpu.VMEM((rows, z.per, local), BF16),
        pltpu.VMEM((rows, z.per, local), BF16),
        pltpu.VMEM((z.nz, local, z.ny * z.blk), BF16),
    ]
    dma = pltpu.SemaphoreType.DMA
    scratch += [dma((6,)), dma, dma, dma, dma, dma, dma((4,)), dma((4,)), dma((4,)), dma((4,)),
                dma, dma, dma, dma, dma, dma, dma((z.nz,))]
    mixed = pl.pallas_call(
        functools.partial(kernel, z),
        out_shape=jax.ShapeDtypeStruct((local, width), BF16),
        in_specs=[any_spec, vmem, vmem] + [any_spec] * 6,
        out_specs=any_spec,
        scratch_shapes=scratch,
        compiler_params=pltpu.CompilerParams(
            collective_id=0, has_side_effects=True, vmem_limit_bytes=60 * 1024 * 1024
        ),
        name="fourier_mix",
    )(tokens[0], norm_gain[None], block, *consts)
    return mixed[None]


def solution(mesh):
    rows, cols = mesh.shape["row"], mesh.shape["col"]
    in_specs = (P("col", "row", None), P(), P("row", "col"), P("col", "row"))
    return jax.shard_map(
        functools.partial(body, rows, cols), mesh=mesh, in_specs=in_specs,
        out_specs=P("col", "row", None), check_vma=False,
    )
```

time: 214 us -> 80 us (0.37)
  the two profiles are of different devices: /device:TPU:4 before, /device:TPU:1 now
where the time goes in v1:
time: 80 us; the launch traced here: 79.7 us
  Pallas kernels  74.3 us (93%)
  local copies, waits for them, and re-layouts  4.02 us (5%)
  other arithmetic  1.39 us (2%)
    pallas_call x1, Pallas kernels, body(): pl.pallas_call(functools.partial(kernel, z), out_shape=jax.ShapeDtypeStru...  74.3 us
    unnamed x1, local copies, waits for them, and re-layouts  2.73 us

profile of v1, /device:TPU:1, one launch (start us, length us, event | category | flops | bytes accessed | tf_op | source)
XLA Modules:
  0.0 79.7 jit_solution(12374731933799716313)
XLA Ops:
  0.0 1.3 %broadcast_in_dim.6.gain_ref = bf16[1,2048]{1,0:T(2,128)(2,1)} reshape(bf16[2048]{0:T(1024)(128)(2,1)} %param.11) | data formatting | bytes 8192 | tf_op jit(solution)/shard_map/broadcast_in_dim | solution.py:370
  1.3 1.4 %pad_maximum_fusion.blk_ref = bf16[32,128]{1,0:T(8,128)(2,1)} fusion(bf16[32,64]{1,0:T(8,128)(2,1)} %bitcast.5, bf16[32,64]{1,0:T(8,128)(2,1)} %param.12), kind=kLoop, calls=%fused_computation | loop fusion | flops 16384 | bytes 16384 | tf_op jit(solution)/shard_map/concatenate | solution.py:339
  2.7 74.3 %fourier_mix.1 = bf16[384,2048]{1,0:T(8,128)(2,1)} custom-call(bf16[384,2048]{1,0:T(8,128)(2,1)} %bitcast.4, bf16[1,2048]{1,0:T(2,128)(2,1)} %broadcast_in_dim.6.gain_ref, bf16[32,128]{1,0:T(8,128)(2,1)} %pad_maximum_fusion.blk_ref, bf16[256,256]{1,0:T(8,128)(2,1)} %constant.21.chan_hbm, bf16[2,256,128]{2,1,0:T(8,128)(2,1)} %constant.22.first_hbm, ...), custom_call_target="tpu_custom_call" | custom-call | tf_op jit(solution)/shard_map/fourier_mix/pallas_call | solution.py:360
  77.0 2.7 %copy.12 = bf16[1,384,2048]{2,1,0:T(8,128)(2,1)} copy(bf16[1,384,2048]{2,1,0:T(8,128)(2,1)} %bitcast.3) | data formatting | bytes 3145728

commit v2 on v1

v2 whole, which is shorter than its diff:
```python
import functools
import math

import jax
import jax.numpy as jnp
import numpy as np
from jax import lax
from jax.experimental import pallas as pl
from jax.experimental.pallas import tpu as pltpu
from jax.sharding import PartitionSpec as P

GS = 64
HALF = GS // 2
EPS = 1e-06
F32 = jnp.float32
BF16 = jnp.bfloat16
MESH = pl.DeviceIdType.MESH
VMEM_LIMIT = 52 * 1024 * 1024


class Sizes:
    def __init__(self, rows, cols, local, width):
        self.rows = rows
        self.nz = 1 << ((rows.bit_length() - 1 + 1) // 2)
        self.ny = rows // self.nz
        self.nx = cols // 2
        self.local = local
        self.width = width
        self.ch = GS * self.nx
        self.per = 2 * self.ch // rows
        self.pairs = self.per // 2
        self.hops = local // rows
        self.blk = width // rows
        self.cut = 4
        self.tiles = max(1, local // 128)
        self.lane = local // self.tiles


def tables(z):
    rows, local, ch = z.rows, z.local, z.ch
    length = rows * local
    k = np.arange(GS)
    small = np.zeros((GS, GS))
    for j in range(HALF):
        if j == 0:
            small[0] = (1.0 + (-1.0) ** k) / 2
            small[1] = (1.0 - (-1.0) ** k) / 2
        else:
            small[2 * j] = np.cos(2 * math.pi * j * k / GS)
            small[2 * j + 1] = np.sin(2 * math.pi * j * k / GS)
    chan = np.kron(np.eye(z.nx), small)
    i = np.arange(rows)
    ang = 2 * math.pi * (np.outer(i, i) % rows) / rows
    c, s = np.cos(ang), np.sin(ang)
    first = np.concatenate(
        [
            np.block([[c, -s], [-s, -c], [c, s], [-s, c]]),
            np.block([[c, c], [-s, -s], [c, -c], [-s, s]]),
        ]
    )
    m = np.arange(local)
    tw = 2 * math.pi * np.outer(i, m) / length
    turn = np.concatenate([np.cos(tw), np.sin(tw)]).astype(np.float32)
    high = turn.astype(BF16).astype(np.float32)
    turn = np.concatenate([high, turn - high], axis=1)
    a = np.arange(z.hops)
    k2 = (z.hops * i[None, :] + a[:, None]).reshape(-1)
    ang2 = 2 * math.pi * (np.outer(k2, m) % local) / local
    second = np.concatenate([np.cos(ang2), np.sin(ang2)], axis=1) / math.sqrt(length * GS)
    parts = []
    for part in (second, first, chan, turn):
        wide = np.zeros((part.shape[0], 2 * local), np.float32)
        wide[:, : part.shape[1]] = part
        parts.append(wide)
    return jnp.asarray(np.concatenate(parts).astype(BF16))


def dot(a, b):
    return jnp.dot(a, b, preferred_element_type=F32)


def dot_nt(a, b):
    return lax.dot_general(a, b, (((1,), (1,)), ((), ())), preferred_element_type=F32)


def placed(rows, cols, target, keep):
    to = lax.broadcasted_iota(jnp.int32, (rows, cols), 1)
    return jnp.where((to == target) & keep, 1.0, 0.0).astype(BF16)


def kernel(
    z,
    tok_hbm, gain_hbm, wi_hbm, wt_hbm, tab_hbm,
    out,
    gain_ref, wi_ref, wt_ref, tab, tok,
    xbuf, win, wpk, wo, spread, ht, got, stage, gp, back, got2,
    tab_sem, tok_sem, swap_send, swap_recv,
    x_send, x_recv, in_send, in_recv, ring_recv, wo_send, wo_recv,
    far_send, far_recv, half_send, half_recv,
    a_send, a_recv, b_send, b_recv,
):
    rows, ny, nz, nx, local = z.rows, z.ny, z.nz, z.nx, z.local
    groups = rows // 2
    r = lax.axis_index("row")
    c = lax.axis_index("col")
    h = lax.rem(c, 2)
    x = c // 2
    zz = r // ny
    yy = lax.rem(r, ny)
    other = c + 1 - 2 * h

    def send(src, dst, ssem, rsem, row, col):
        copy = pltpu.make_async_remote_copy(
            src_ref=src, dst_ref=dst, send_sem=ssem, recv_sem=rsem,
            device_id=(row, col), device_id_type=MESH,
        )
        copy.start()

    def drain(ref, sem):
        pltpu.make_async_copy(ref, ref, sem).wait()

    barrier = pltpu.get_barrier_semaphore()
    loads = [
        pltpu.make_async_copy(src, dst, tab_sem.at[n])
        for n, (src, dst) in enumerate(
            [(wi_hbm, wi_ref), (wt_hbm, wt_ref), (gain_hbm, gain_ref), (tab_hbm, tab)]
        )
    ]
    for load in loads[:2]:
        load.start()

    def greet(i, carry):
        peer = lax.rem(r + i, rows)
        pl.semaphore_signal(barrier, inc=1, device_id=(peer, c), device_id_type=MESH)
        pl.semaphore_signal(barrier, inc=1, device_id=(peer, other), device_id_type=MESH)
        return carry

    for d in range(1, nx):
        px = lax.rem(x + d, nx)
        pl.semaphore_signal(barrier, inc=1, device_id=(r, 2 * px + h), device_id_type=MESH)
    pl.semaphore_signal(barrier, inc=1, device_id=(r, other), device_id_type=MESH)
    lax.fori_loop(1, rows, greet, 0)

    own = pltpu.make_async_copy(tok_hbm, tok.at[h], tok_sem)
    own.start()
    for load in loads[2:]:
        load.start()
    packed = 2 * GS
    at = lax.broadcasted_iota(jnp.int32, (nx * packed, z.ch), 0)
    for half in range(2):
        q = lax.rem(at, packed) - GS * half
        place = jnp.where(q < HALF, 2 * q, 2 * GS + 1 - 2 * q)
        place = jnp.where(q == HALF, 1, place) + GS * (at // packed)
        spread[half] = placed(nx * packed, z.ch, place, (q >= 0) & (q < GS))
    loads[0].wait()
    loads[1].wait()
    hb = z.blk // 2
    lo, hi = pl.ds(0, hb), pl.ds(hb, hb)
    side = lax.broadcasted_iota(jnp.int32, (GS, packed), 0)
    everywhere = side >= 0
    wpk[h, x, zz, yy] = (
        dot(wt_ref[:hb], placed(GS, packed, side, everywhere))
        + dot(wt_ref[hb:], placed(GS, packed, side + GS, everywhere))
    ).astype(BF16)
    xbuf[x] = wi_ref[...]
    pl.semaphore_wait(barrier, 2 * rows - 1 + nx - 1)

    for d in range(1, nx):
        px = lax.rem(x + d, nx)
        send(wi_ref, xbuf.at[x], x_send, x_recv, r, 2 * px + h)
    send(tok_hbm, tok.at[h], swap_send, swap_recv, r, other)
    chan_at = lax.broadcasted_iota(jnp.int32, (GS, z.ch), 0)
    drain(xbuf.at[pl.ds(0, nx - 1)], x_recv)
    total = dot(xbuf[0], placed(GS, z.ch, chan_at, chan_at >= 0))
    for n in range(1, nx):
        total += dot(xbuf[n], placed(GS, z.ch, chan_at + GS * n, chan_at >= 0))
    win[zz, yy] = total.astype(BF16)

    for d in range(1, ny):
        py = lax.rem(yy + d, ny)
        send(win.at[zz, yy, lo], win.at[zz, yy, lo], in_send.at[0], in_recv.at[0], zz * ny + py, c)
    for d in range(1, nz):
        pz = lax.rem(zz + d, nz)
        send(win.at[zz, yy, hi], win.at[zz, yy, hi], in_send.at[1], in_recv.at[1], pz * ny + yy, c)
    mine = wpk.at[h, x]

    @pl.when(h == 0)
    def _():
        for d in range(1, ny):
            py = lax.rem(yy + d, ny)
            send(mine.at[zz, yy], mine.at[zz, yy], wo_send.at[0], wo_recv.at[0], zz * ny + py, c)

    @pl.when(h == 1)
    def _():
        for d in range(1, nz):
            pz = lax.rem(zz + d, nz)
            send(mine.at[zz, yy], mine.at[zz, yy], wo_send.at[0], wo_recv.at[0], pz * ny + yy, c)

    loads[2].wait()
    gain = gain_ref[...].astype(F32).reshape(1, z.width)
    step = min(32, local)

    def norm(q):
        def one(i, carry):
            part = pl.ds(pl.multiple_of(i * step, step), step)
            v = tok[q, part, :].astype(F32)
            inv = lax.rsqrt(jnp.mean(v * v, axis=-1, keepdims=True) + EPS)
            tok[q, part, :] = (v * inv * gain).astype(BF16)
            return carry

        lax.fori_loop(0, local // step, one, 0)

    own.wait()
    norm(h)

    drain(win.at[0, pl.ds(0, ny - 1), lo], in_recv.at[0])
    drain(win.at[pl.ds(0, nz - 1), 0, hi], in_recv.at[1])
    cy, cz = min(z.cut, ny), min(z.cut, nz)

    def low(block, chunk):
        return win.at[block, pl.ds(chunk * (ny // cy), ny // cy), lo]

    def high(block, chunk):
        return win.at[pl.ds(chunk * (nz // cz), nz // cz), block, hi]

    def row_z(p):
        return p * ny + yy

    def row_y(p):
        return zz * ny + p

    paths = ((low, nz, zz, cy, row_z), (high, ny, yy, cz, row_y))

    def carried(n, cut, hop, sign):
        if hop < n // 2:
            return range(cut)
        return range(cut // 2) if sign > 0 else range(cut // 2, cut)

    longest = max(nz, ny) // 2

    def advance(hop):
        for chunk in range(max(cy, cz)):
            for p, (view, n, pos, cut, row) in enumerate(paths):
                for e, sign in enumerate((1, -1)):
                    block = lax.rem(pos - sign * (hop - 1) + n, n)
                    if 1 < hop <= n // 2 + 1 and chunk in carried(n, cut, hop - 1, sign):
                        drain(view(block, chunk), ring_recv.at[p, e, hop - 2, chunk])
                    if hop <= n // 2 and chunk in carried(n, cut, hop, sign):
                        to = lax.rem(pos + sign + n, n)
                        send(view(block, chunk), view(block, chunk), in_send.at[2 + p],
                             ring_recv.at[p, e, hop - 1, chunk], row(to), c)

    advance(1)

    @pl.when(h == 0)
    def _():
        drain(wpk.at[0, 0, 0, pl.ds(0, ny - 1)], wo_recv.at[0])
        for d in range(1, nz):
            pz = lax.rem(zz + d, nz)
            send(mine.at[zz], mine.at[zz], wo_send.at[1], wo_recv.at[1], pz * ny + yy, c)

    @pl.when(h == 1)
    def _():
        drain(wpk.at[0, 0, pl.ds(0, nz - 1), 0], wo_recv.at[0])
        for d in range(1, ny):
            py = lax.rem(yy + d, ny)
            send(mine.at[:, yy], mine.at[:, yy], wo_send.at[1], wo_recv.at[1], zz * ny + py, c)

    drain(tok.at[0], swap_recv)
    norm(1 - h)
    for hop in range(2, longest + 2):
        with jax.named_scope(f"pring{hop}"):
            advance(hop)

    @pl.when(h == 0)
    def _():
        drain(wpk.at[0, 0, pl.ds(0, nz - 1)], wo_recv.at[1])

    @pl.when(h == 1)
    def _():
        drain(wpk.at[0, 0, :, pl.ds(0, ny - 1)], wo_recv.at[1])

    near = (1, nx - 1) if nx == 4 else tuple(range(1, nx))
    for n, d in enumerate(near):
        px = lax.rem(x + d, nx)
        send(mine, mine, far_send, far_recv.at[n], r, 2 * px + h)
    send(mine, mine, half_send, half_recv.at[0], r, other)

    loads[3].wait()
    o1 = local
    o2 = o1 + 8 * rows
    o3 = o2 + z.ch
    chan = tab[o2:o3, :z.ch]
    weight = win[...].reshape(z.width, z.ch)
    for q in range(2):
        proj = dot(tok[q], weight).astype(BF16)
        cols = dot_nt(chan, proj).astype(BF16)
        ht[pl.ds(groups * q, groups)] = cols.reshape(groups, z.per, local)

        def scatter(i, carry):
            peer = groups * q + lax.rem(r + i, groups)

            @pl.when(peer != r)
            def _():
                send(ht.at[peer], got.at[r], a_send, a_recv, peer, c)

            return carry

        lax.fori_loop(0, groups, scatter, 0)
    got[r] = ht[r]

    zh = nz // 2
    for n, d in enumerate(near):
        theirs = wpk.at[h, lax.rem(x - d + nx, nx)]
        drain(theirs, far_recv.at[n])
        if nx == 4:
            part = pl.ds(n * zh, zh)
            to = lax.rem(x + d, nx)
            send(theirs.at[part], theirs.at[part], far_send, far_recv.at[2 + n], r, 2 * to + h)
        send(theirs, theirs, half_send, half_recv.at[1 + n], r, other)

    drain(got.at[pl.ds(0, rows - 1)], a_recv)

    lane = z.lane
    for l in range(z.tiles):
        part = got[:, :, l * lane:(l + 1) * lane].astype(F32)
        stage[l] = part.reshape(rows * z.per, lane)
    base = lax.rem(r, groups) * z.pairs
    plain = tab[o1:o1 + 4 * rows, :2 * rows]
    for p in range(z.pairs):
        matrix = plain
        if p % min(z.pairs, HALF) == 0:
            paired = tab[o1 + 4 * rows:o2, :2 * rows].astype(F32)
            special = lax.rem(base + p, HALF) == 0
            matrix = jnp.where(special, paired, plain.astype(F32)).astype(BF16)
        for l in range(z.tiles):
            lanes = slice(l * lane, (l + 1) * lane)
            rest = slice(local + l * lane, local + (l + 1) * lane)
            cos = tab[o3:o3 + rows, lanes].astype(F32) + tab[o3:o3 + rows, rest].astype(F32)
            sin = (tab[o3 + rows:o3 + 2 * rows, lanes].astype(F32)
                   + tab[o3 + rows:o3 + 2 * rows, rest].astype(F32))
            u = stage[l, pl.ds(2 * p, rows, stride=z.per), :]
            v = stage[l, pl.ds(2 * p + 1, rows, stride=z.per), :]
            g = dot(matrix, jnp.concatenate([u, v], axis=0).astype(BF16))
            for w in range(2):
                re = g[2 * w * rows:(2 * w + 1) * rows]
                im = g[(2 * w + 1) * rows:(2 * w + 2) * rows]
                at = pl.ds((2 * p + w) * rows, rows)
                gp[at, lanes] = (re * cos + im * sin).astype(BF16)
                gp[at, rest] = (im * cos - re * sin).astype(BF16)
    spec = dot_nt(tab[:local], gp[...])
    if rows == GS and lane == 128:
        left = lax.broadcasted_iota(jnp.int32, (rows, lane), 1) < rows
        for l in range(z.tiles):
            for p in range(z.pairs):
                t0 = spec[2 * l * rows:(2 * l + 1) * rows, p * lane:(p + 1) * lane]
                t1 = spec[(2 * l + 1) * rows:(2 * l + 2) * rows, p * lane:(p + 1) * lane]
                stage[l, pl.ds(2 * p, rows, stride=z.per), :] = jnp.where(
                    left, t0, pltpu.roll(t1, rows, 1)
                )
                stage[l, pl.ds(2 * p + 1, rows, stride=z.per), :] = jnp.where(
                    left, pltpu.roll(t0, rows, 1), t1
                )
    else:
        full = spec.reshape(z.hops, rows, z.per, rows).transpose(1, 2, 0, 3)
        full = full.reshape(rows * z.per, z.tiles, lane)
        for l in range(z.tiles):
            stage[l] = full[:, l]
    for l in range(z.tiles):
        back[:, :, l * lane:(l + 1) * lane] = stage[l].reshape(rows, z.per, lane).astype(BF16)

    seq = r // groups
    slot = h * groups + lax.rem(r, groups)
    target = 2 * x + seq

    def give(i, carry):
        peer = lax.rem(r + i, rows)
        send(back.at[peer], got2.at[slot], b_send, b_recv, peer, target)
        return carry

    lax.fori_loop(1, rows, give, 0)

    @pl.when(seq == h)
    def _():
        got2[slot] = back[r]

    @pl.when(seq != h)
    def _():
        send(back.at[r], got2.at[slot], b_send, b_recv, r, target)

    if nx == 4:
        far = lax.rem(x + 2, nx)
        for n in range(2):
            part = wpk.at[h, far, pl.ds(n * zh, zh)]
            drain(part, far_recv.at[2 + n])
            send(part, part, half_send, half_recv.at[3], r, other)

    def unpack(half_of):
        flat = jnp.concatenate(
            [wpk[half_of, n].reshape(rows * hb, packed) for n in range(nx)], axis=1
        )
        for half in range(2):
            sorted_ = dot(flat, spread[half]).astype(BF16)
            wo[half_of, :, half * hb:(half + 1) * hb, :] = sorted_.reshape(rows, hb, z.ch)

    unpack(h)
    for n in range(nx):
        drain(wpk.at[0, 0], half_recv.at[n])
    unpack(1 - h)

    @pl.when(seq == h)
    def _():
        drain(got2.at[pl.ds(0, rows - 1)], b_recv)

    @pl.when(seq != h)
    def _():
        drain(got2, b_recv)

    mixed = got2[...].astype(F32).reshape(rows * z.per, local).T.astype(BF16)
    ma, mb = mixed[:, :z.ch], mixed[:, z.ch:]
    chunk = ny * z.blk
    for n in range(nz):
        some = pl.ds(n * ny, ny)
        res = dot_nt(ma, wo[0, some].reshape(chunk, z.ch)) + dot_nt(mb, wo[1, some].reshape(chunk, z.ch))
        out[:, n * chunk:(n + 1) * chunk] = res.astype(BF16)

    drain(xbuf.at[pl.ds(0, nx - 1)], x_send)
    drain(tok.at[0], swap_send)
    drain(win.at[0, pl.ds(0, ny - 1), lo], in_send.at[0])
    drain(win.at[pl.ds(0, nz - 1), 0, hi], in_send.at[1])
    drain(win.at[pl.ds(0, nz - 1), :, lo], in_send.at[2])
    drain(win.at[:, pl.ds(0, ny - 1), hi], in_send.at[3])

    @pl.when(h == 0)
    def _():
        drain(wpk.at[0, 0, 0, pl.ds(0, ny - 1)], wo_send.at[0])
        drain(wpk.at[0, 0, pl.ds(0, nz - 1)], wo_send.at[1])

    @pl.when(h == 1)
    def _():
        drain(wpk.at[0, 0, pl.ds(0, nz - 1), 0], wo_send.at[0])
        drain(wpk.at[0, 0, :, pl.ds(0, ny - 1)], wo_send.at[1])

    drain(wpk.at[0, pl.ds(0, nx - 1)], far_send)
    drain(wpk.at[0], half_send)
    drain(ht.at[pl.ds(0, rows - 1)], a_send)

    @pl.when(seq == h)
    def _():
        drain(back.at[pl.ds(0, rows - 1)], b_send)

    @pl.when(seq != h)
    def _():
        drain(back, b_send)


def body(rows, cols, tokens, norm_gain, in_weight, out_weight):
    local, width = tokens.shape[1:]
    z = Sizes(rows, cols, local, width)
    table = tables(z)
    hbm = pl.BlockSpec(memory_space=pltpu.HBM)
    vmem = pl.BlockSpec(memory_space=pltpu.VMEM)
    hb = z.blk // 2
    dma = pltpu.SemaphoreType.DMA
    vm = pltpu.VMEM
    exchange = (rows, z.per, local)
    scratch = [
        vm((width,), BF16),
        vm((z.blk, GS), BF16),
        vm((z.blk, GS), BF16),
        vm(table.shape, BF16),
        vm((2, local, width), BF16),
        vm((z.nx, z.blk, GS), BF16),
        vm((z.nz, z.ny, z.blk, z.ch), BF16),
        vm((2, z.nx, z.nz, z.ny, hb, 2 * GS), BF16),
        vm((2, rows, z.blk, z.ch), BF16),
        vm((2, 2 * GS * z.nx, z.ch), BF16),
        vm(exchange, BF16),
        vm(exchange, BF16),
        vm((z.tiles, rows * z.per, z.lane), F32),
        vm((z.per * rows, 2 * local), BF16),
        vm(exchange, BF16),
        vm(exchange, BF16),
        dma((4,)), dma, dma, dma,
        dma, dma, dma((4,)), dma((2,)), dma((2, 2, max(z.ny, z.nz) // 2, z.cut)), dma((2,)), dma((2,)),
        dma, dma((4,)), dma, dma((4,)),
        dma, dma, dma, dma,
    ]
    operands = (tokens[0], norm_gain, in_weight, out_weight.T, table)
    mixed = pl.pallas_call(
        functools.partial(kernel, z),
        out_shape=jax.ShapeDtypeStruct((local, width), BF16),
        in_specs=[hbm] * 5,
        out_specs=vmem,
        scratch_shapes=scratch,
        compiler_params=pltpu.CompilerParams(
            collective_id=0, has_side_effects=True, vmem_limit_bytes=VMEM_LIMIT
        ),
        name="fourier_mix",
    )(*(pltpu.with_memory_space_constraint(a, pltpu.HBM) for a in operands))
    return mixed[None]


def solution(mesh):
    rows, cols = mesh.shape["row"], mesh.shape["col"]
    in_specs = (P("col", "row", None), P(), P("row", "col"), P("col", "row"))
    return jax.shard_map(
        functools.partial(body, rows, cols), mesh=mesh, in_specs=in_specs,
        out_specs=P("col", "row", None), check_vma=False,
    )
```

time: 80 us -> 70 us (0.88); the launches traced: 79.7 us -> 68.6 us
  Pallas kernels: 74.3 us -> 67.5 us
  local copies, waits for them, and re-layouts: 4.02 us -> 1.15 us
  other arithmetic: 1.39 us -> 0 us
    pallas_call x1, Pallas kernels: 74.3 us -> 67.5 us  [body(): pl.pallas_call(functools.partial(kernel, z), out_shape=jax.ShapeDtypeStru...]
    unnamed x1, local copies, waits for them, and re-layouts: 2.73 us -> 1.15 us
    concatenate x1 -> x0, other arithmetic: 1.39 us -> none  [body(): block = jnp.concatenate([in_weight, out_weight.T], axis=1)]
    broadcast_in_dim x1 -> x0, local copies, waits for them, and re-layouts: 1.29 us -> none  [body(): norm_gain[None]]
where the time goes in v2:
time: 70 us; the launch traced here: 68.6 us
  Pallas kernels  67.5 us (96%)
  local copies, waits for them, and re-layouts  1.15 us (2%)
    pallas_call x1, Pallas kernels, body(): pl.pallas_call(functools.partial(kernel, z), out_shape=jax.ShapeDtypeStru...  67.5 us

profile of v2, /device:TPU:1, one launch (start us, length us, event | category | flops | bytes accessed | tf_op | source)
XLA Modules:
  0.0 68.6 jit_solution(11220541363627628807)
XLA Ops:
  0.0 67.5 %fourier_mix.1 = bf16[384,2048]{1,0:T(8,128)(2,1)S(1)} custom-call(bf16[384,2048]{1,0:T(8,128)(2,1)} %bitcast.4, bf16[2048]{0:T(1024)(128)(2,1)} %gain_hbm.1, bf16[32,64]{1,0:T(8,128)(2,1)} %wi_hbm.1, bf16[32,64]{1,0:T(8,128)(2,1)} %bitcast.5, bf16[1280,768]{1,0:T(8,128)(2,1)} %constant.2.clone.tab_hbm), custom_call_target="tpu_custom_call" | custom-call | tf_op jit(solution)/shard_map/fourier_mix/pallas_call | solution.py:490
  67.5 1.1 %copy.7 = bf16[1,384,2048]{2,1,0:T(8,128)(2,1)} copy(bf16[1,384,2048]{2,1,0:T(8,128)(2,1)S(1)} %bitcast.3) | data formatting | bytes 3145728

commit v3 on v2

--- a/solution.py
+++ b/solution.py
@@ -97,7 +97,7 @@
     tab_sem, tok_sem, swap_send, swap_recv,
     x_send, x_recv, in_send, in_recv, ring_recv, wo_send, wo_recv,
     far_send, far_recv, half_send, half_recv,
-    a_send, a_recv, b_send, b_recv,
+    a_send, a_recv, b_send, b_recv, plane_sem,
 ):
     rows, ny, nz, nx, local = z.rows, z.ny, z.nz, z.nx, z.local
     groups = rows // 2
@@ -129,17 +129,16 @@
     for load in loads[:2]:
         load.start()
 
-    def greet(i, carry):
-        peer = lax.rem(r + i, rows)
-        pl.semaphore_signal(barrier, inc=1, device_id=(peer, c), device_id_type=MESH)
-        pl.semaphore_signal(barrier, inc=1, device_id=(peer, other), device_id_type=MESH)
-        return carry
-
     for d in range(1, nx):
         px = lax.rem(x + d, nx)
         pl.semaphore_signal(barrier, inc=1, device_id=(r, 2 * px + h), device_id_type=MESH)
+    for d in range(1, ny):
+        to = zz * ny + lax.rem(yy + d, ny)
+        pl.semaphore_signal(barrier, inc=1, device_id=(to, c), device_id_type=MESH)
+    for d in range(1, nz):
+        to = lax.rem(zz + d, nz) * ny + yy
+        pl.semaphore_signal(barrier, inc=1, device_id=(to, c), device_id_type=MESH)
     pl.semaphore_signal(barrier, inc=1, device_id=(r, other), device_id_type=MESH)
-    lax.fori_loop(1, rows, greet, 0)
 
     own = pltpu.make_async_copy(tok_hbm, tok.at[h], tok_sem)
     own.start()
@@ -163,12 +162,26 @@
         + dot(wt_ref[hb:], placed(GS, packed, side + GS, everywhere))
     ).astype(BF16)
     xbuf[x] = wi_ref[...]
-    pl.semaphore_wait(barrier, 2 * rows - 1 + nx - 1)
+    pl.semaphore_wait(barrier, nx + ny + nz - 2)
 
     for d in range(1, nx):
         px = lax.rem(x + d, nx)
         send(wi_ref, xbuf.at[x], x_send, x_recv, r, 2 * px + h)
     send(tok_hbm, tok.at[h], swap_send, swap_recv, r, other)
+    mine = wpk.at[h, x]
+
+    @pl.when(h == 0)
+    def _():
+        for d in range(1, ny):
+            py = lax.rem(yy + d, ny)
+            send(mine.at[zz, yy], mine.at[zz, yy], wo_send.at[0], wo_recv.at[0], zz * ny + py, c)
+
+    @pl.when(h == 1)
+    def _():
+        for d in range(1, nz):
+            pz = lax.rem(zz + d, nz)
+            send(mine.at[zz, yy], mine.at[zz, yy], wo_send.at[0], wo_recv.at[0], pz * ny + yy, c)
+
     chan_at = lax.broadcasted_iota(jnp.int32, (GS, z.ch), 0)
     drain(xbuf.at[pl.ds(0, nx - 1)], x_recv)
     total = dot(xbuf[0], placed(GS, z.ch, chan_at, chan_at >= 0))
@@ -182,20 +195,6 @@
     for d in range(1, nz):
         pz = lax.rem(zz + d, nz)
         send(win.at[zz, yy, hi], win.at[zz, yy, hi], in_send.at[1], in_recv.at[1], pz * ny + yy, c)
-    mine = wpk.at[h, x]
-
-    @pl.when(h == 0)
-    def _():
-        for d in range(1, ny):
-            py = lax.rem(yy + d, ny)
-            send(mine.at[zz, yy], mine.at[zz, yy], wo_send.at[0], wo_recv.at[0], zz * ny + py, c)
-
-    @pl.when(h == 1)
-    def _():
-        for d in range(1, nz):
-            pz = lax.rem(zz + d, nz)
-            send(mine.at[zz, yy], mine.at[zz, yy], wo_send.at[0], wo_recv.at[0], pz * ny + yy, c)
-
     loads[2].wait()
     gain = gain_ref[...].astype(F32).reshape(1, z.width)
     step = min(32, local)
@@ -272,6 +271,8 @@
         with jax.named_scope(f"pring{hop}"):
             advance(hop)
 
+    pl.semaphore_signal(plane_sem, inc=1, device_id=(r, other), device_id_type=MESH)
+
     @pl.when(h == 0)
     def _():
         drain(wpk.at[0, 0, pl.ds(0, nz - 1)], wo_recv.at[1])
@@ -320,6 +321,13 @@
         send(theirs, theirs, half_send, half_recv.at[1 + n], r, other)
 
     drain(got.at[pl.ds(0, rows - 1)], a_recv)
+
+    if nx == 4:
+        far = lax.rem(x + 2, nx)
+        for n in range(2):
+            part = wpk.at[h, far, pl.ds(n * zh, zh)]
+            drain(part, far_recv.at[2 + n])
+            send(part, part, half_send, half_recv.at[3], r, other)
 
     lane = z.lane
     for l in range(z.tiles):
@@ -369,6 +377,7 @@
     for l in range(z.tiles):
         back[:, :, l * lane:(l + 1) * lane] = stage[l].reshape(rows, z.per, lane).astype(BF16)
 
+    pl.semaphore_wait(plane_sem, 1)
     seq = r // groups
     slot = h * groups + lax.rem(r, groups)
     target = 2 * x + seq
@@ -387,13 +396,6 @@
     @pl.when(seq != h)
     def _():
         send(back.at[r], got2.at[slot], b_send, b_recv, r, target)
-
-    if nx == 4:
-        far = lax.rem(x + 2, nx)
-        for n in range(2):
-            part = wpk.at[h, far, pl.ds(n * zh, zh)]
-            drain(part, far_recv.at[2 + n])
-            send(part, part, half_send, half_recv.at[3], r, other)
 
     def unpack(half_of):
         flat = jnp.concatenate(
@@ -484,7 +486,7 @@
         dma((4,)), dma, dma, dma,
         dma, dma, dma((4,)), dma((2,)), dma((2, 2, max(z.ny, z.nz) // 2, z.cut)), dma((2,)), dma((2,)),
         dma, dma((4,)), dma, dma((4,)),
-        dma, dma, dma, dma,
+        dma, dma, dma, dma, pltpu.SemaphoreType.REGULAR,
     ]
     operands = (tokens[0], norm_gain, in_weight, out_weight.T, table)
     mixed = pl.pallas_call(

time: 70 us -> 67.7 us (0.967); the launches traced: 68.6 us -> 67.6 us
  Pallas kernels: 67.5 us -> 66.4 us
    pallas_call x1, Pallas kernels: 67.5 us -> 66.4 us  [body(): pl.pallas_call(functools.partial(kernel, z), out_shape=jax.ShapeDtypeStru...]
where the time goes in v3:
time: 67.7 us; the launch traced here: 67.6 us
  Pallas kernels  66.4 us (98%)
  local copies, waits for them, and re-layouts  1.15 us (2%)
    pallas_call x1, Pallas kernels, body(): pl.pallas_call(functools.partial(kernel, z), out_shape=jax.ShapeDtypeStru...  66.4 us

profile of v3, /device:TPU:1, one launch (start us, length us, event | category | flops | bytes accessed | tf_op | source)
XLA Modules:
  0.0 67.6 jit_solution(5350197790143133663)
XLA Ops:
  0.0 66.4 %fourier_mix.1 = bf16[384,2048]{1,0:T(8,128)(2,1)S(1)} custom-call(bf16[384,2048]{1,0:T(8,128)(2,1)} %bitcast.4, bf16[2048]{0:T(1024)(128)(2,1)} %gain_hbm.1, bf16[32,64]{1,0:T(8,128)(2,1)} %wi_hbm.1, bf16[32,64]{1,0:T(8,128)(2,1)} %bitcast.5, bf16[1280,768]{1,0:T(8,128)(2,1)} %constant.2.clone.tab_hbm), custom_call_target="tpu_custom_call" | custom-call | tf_op jit(solution)/shard_map/fourier_mix/pallas_call | solution.py:492
  66.5 1.1 %copy.7 = bf16[1,384,2048]{2,1,0:T(8,128)(2,1)} copy(bf16[1,384,2048]{2,1,0:T(8,128)(2,1)S(1)} %bitcast.3) | data formatting | bytes 3145728

commit v4 on v3

--- a/solution.py
+++ b/solution.py
@@ -212,6 +212,20 @@
     own.wait()
     norm(h)
 
+    @pl.when(h == 0)
+    def _():
+        drain(wpk.at[0, 0, 0, pl.ds(0, ny - 1)], wo_recv.at[0])
+        for d in range(1, nz):
+            pz = lax.rem(zz + d, nz)
+            send(mine.at[zz], mine.at[zz], wo_send.at[1], wo_recv.at[1], pz * ny + yy, c)
+
+    @pl.when(h == 1)
+    def _():
+        drain(wpk.at[0, 0, pl.ds(0, nz - 1), 0], wo_recv.at[0])
+        for d in range(1, ny):
+            py = lax.rem(yy + d, ny)
+            send(mine.at[:, yy], mine.at[:, yy], wo_send.at[1], wo_recv.at[1], zz * ny + py, c)
+
     drain(win.at[0, pl.ds(0, ny - 1), lo], in_recv.at[0])
     drain(win.at[pl.ds(0, nz - 1), 0, hi], in_recv.at[1])
     cy, cz = min(z.cut, ny), min(z.cut, nz)
@@ -236,6 +250,36 @@
         return range(cut // 2) if sign > 0 else range(cut // 2, cut)
 
     longest = max(nz, ny) // 2
+    line8 = nz == 8 and ny == 8
+
+    def hand(view, chunk, block, p, e, kind, to, row):
+        send(view(block, chunk), view(block, chunk), in_send.at[2 + p],
+             ring_recv.at[p, e, kind, chunk], row(to), c)
+
+    def start8():
+        for chunk in range(z.cut):
+            for far in (2, 1):
+                for p, (view, n, pos, cut, row) in enumerate(paths):
+                    for e, sign in enumerate((1, -1)):
+                        hand(view, chunk, pos, p, e, far - 1, lax.rem(pos + far * sign + n, n), row)
+
+    def relay8():
+        for chunk in range(z.cut):
+            for p, (view, n, pos, cut, row) in enumerate(paths):
+                for e, sign in enumerate((1, -1)):
+                    block = lax.rem(pos - 2 * sign + n, n)
+                    drain(view(block, chunk), ring_recv.at[p, e, 1, chunk])
+                    hand(view, chunk, block, p, e, 2, lax.rem(pos + sign + n, n), row)
+                    if chunk in carried(n, cut, n // 2, sign):
+                        hand(view, chunk, block, p, e, 3, lax.rem(pos + 2 * sign + n, n), row)
+
+    def finish8():
+        for kind in (0, 2, 3):
+            for chunk in range(z.cut):
+                for p, (view, n, pos, cut, row) in enumerate(paths):
+                    for e, sign in enumerate((1, -1)):
+                        if kind < 3 or chunk in carried(n, cut, n // 2, sign):
+                            drain(view(pos, chunk), ring_recv.at[p, e, kind, chunk])
 
     def advance(hop):
         for chunk in range(max(cy, cz)):
@@ -249,26 +293,20 @@
                         send(view(block, chunk), view(block, chunk), in_send.at[2 + p],
                              ring_recv.at[p, e, hop - 1, chunk], row(to), c)
 
-    advance(1)
-
-    @pl.when(h == 0)
-    def _():
-        drain(wpk.at[0, 0, 0, pl.ds(0, ny - 1)], wo_recv.at[0])
-        for d in range(1, nz):
-            pz = lax.rem(zz + d, nz)
-            send(mine.at[zz], mine.at[zz], wo_send.at[1], wo_recv.at[1], pz * ny + yy, c)
-
-    @pl.when(h == 1)
-    def _():
-        drain(wpk.at[0, 0, pl.ds(0, nz - 1), 0], wo_recv.at[0])
-        for d in range(1, ny):
-            py = lax.rem(yy + d, ny)
-            send(mine.at[:, yy], mine.at[:, yy], wo_send.at[1], wo_recv.at[1], zz * ny + py, c)
+    if line8:
+        start8()
+    else:
+        advance(1)
 
     drain(tok.at[0], swap_recv)
     norm(1 - h)
-    for hop in range(2, longest + 2):
-        with jax.named_scope(f"pring{hop}"):
+    if line8:
+        with jax.named_scope("pring2"):
+            relay8()
+        with jax.named_scope("pring3"):
+            finish8()
+    else:
+        for hop in range(2, longest + 2):
             advance(hop)
 
     pl.semaphore_signal(plane_sem, inc=1, device_id=(r, other), device_id_type=MESH)
@@ -382,12 +420,19 @@
     slot = h * groups + lax.rem(r, groups)
     target = 2 * x + seq
 
-    def give(i, carry):
-        peer = lax.rem(r + i, rows)
-        send(back.at[peer], got2.at[slot], b_send, b_recv, peer, target)
-        return carry
-
-    lax.fori_loop(1, rows, give, 0)
+    for k in range(nz):
+        pz = k // 2 + (k % 2) * (nz // 2)
+
+        def give(i, carry, pz=pz):
+            peer = pz * ny + lax.rem(yy + i, ny)
+            send(back.at[peer], got2.at[slot], b_send, b_recv, peer, target)
+            return carry
+
+        lax.fori_loop(1, ny, give, 0)
+
+        @pl.when(pz != zz)
+        def _(pz=pz, give=give):
+            give(0, 0)
 
     @pl.when(seq == h)
     def _():

time: 67.7 us -> 60.8 us (0.90)
  Pallas kernels: 66.4 us -> 59.6 us
    pallas_call x1, Pallas kernels: 66.4 us -> 59.6 us  [body(): pl.pallas_call(functools.partial(kernel, z), out_shape=jax.ShapeDtypeStru...]
where the time goes in v4:
time: 60.8 us; the launch traced here: 60.7 us
  Pallas kernels  59.6 us (98%)
  local copies, waits for them, and re-layouts  1.15 us (2%)
    pallas_call x1, Pallas kernels, body(): pl.pallas_call(functools.partial(kernel, z), out_shape=jax.ShapeDtypeStru...  59.6 us

profile of v4, /device:TPU:1, one launch (start us, length us, event | category | flops | bytes accessed | tf_op | source)
XLA Modules:
  0.0 60.7 jit_solution(13990949855720304625)
XLA Ops:
  0.0 59.6 %fourier_mix.1 = bf16[384,2048]{1,0:T(8,128)(2,1)S(1)} custom-call(bf16[384,2048]{1,0:T(8,128)(2,1)} %bitcast.4, bf16[2048]{0:T(1024)(128)(2,1)} %gain_hbm.1, bf16[32,64]{1,0:T(8,128)(2,1)} %wi_hbm.1, bf16[32,64]{1,0:T(8,128)(2,1)} %bitcast.5, bf16[1280,768]{1,0:T(8,128)(2,1)} %constant.2.clone.tab_hbm), custom_call_target="tpu_custom_call" | custom-call | tf_op jit(solution)/shard_map/fourier_mix/pallas_call | solution.py:537
  59.6 1.1 %copy.7 = bf16[1,384,2048]{2,1,0:T(8,128)(2,1)} copy(bf16[1,384,2048]{2,1,0:T(8,128)(2,1)S(1)} %bitcast.3) | data formatting | bytes 3145728

commit v5 on v4

--- a/solution.py
+++ b/solution.py
@@ -331,7 +331,7 @@
     o3 = o2 + z.ch
     chan = tab[o2:o3, :z.ch]
     weight = win[...].reshape(z.width, z.ch)
-    for q in range(2):
+    for q in (1, 0):
         proj = dot(tok[q], weight).astype(BF16)
         cols = dot_nt(chan, proj).astype(BF16)
         ht[pl.ds(groups * q, groups)] = cols.reshape(groups, z.per, local)

time: 60.8 us -> 58.4 us (0.961)
  Pallas kernels: 59.6 us -> 57.1 us
    pallas_call x1, Pallas kernels: 59.6 us -> 57.1 us  [body(): pl.pallas_call(functools.partial(kernel, z), out_shape=jax.ShapeDtypeStru...]
where the time goes in v5:
time: 58.4 us; the launch traced here: 58.3 us
  Pallas kernels  57.1 us (98%)
  local copies, waits for them, and re-layouts  1.15 us (2%)
    pallas_call x1, Pallas kernels, body(): pl.pallas_call(functools.partial(kernel, z), out_shape=jax.ShapeDtypeStru...  57.1 us

profile of v5, /device:TPU:1, one launch (start us, length us, event | category | flops | bytes accessed | tf_op | source)
XLA Modules:
  0.0 58.3 jit_solution(11254888905281463697)
XLA Ops:
  0.0 57.1 %fourier_mix.1 = bf16[384,2048]{1,0:T(8,128)(2,1)S(1)} custom-call(bf16[384,2048]{1,0:T(8,128)(2,1)} %bitcast.4, bf16[2048]{0:T(1024)(128)(2,1)} %gain_hbm.1, bf16[32,64]{1,0:T(8,128)(2,1)} %wi_hbm.1, bf16[32,64]{1,0:T(8,128)(2,1)} %bitcast.5, bf16[1280,768]{1,0:T(8,128)(2,1)} %constant.2.clone.tab_hbm), custom_call_target="tpu_custom_call" | custom-call | tf_op jit(solution)/shard_map/fourier_mix/pallas_call | solution.py:537
  57.1 1.1 %copy.7 = bf16[1,384,2048]{2,1,0:T(8,128)(2,1)} copy(bf16[1,384,2048]{2,1,0:T(8,128)(2,1)S(1)} %bitcast.3) | data formatting | bytes 3145728

commit v6 on v5

--- a/solution.py
+++ b/solution.py
@@ -64,7 +64,8 @@
     high = turn.astype(BF16).astype(np.float32)
     turn = np.concatenate([high, turn - high], axis=1)
     a = np.arange(z.hops)
-    k2 = (z.hops * i[None, :] + a[:, None]).reshape(-1)
+    k2 = z.hops * i.reshape(2, 1, rows // 2) + a[None, :, None]
+    k2 = k2.reshape(-1)
     ang2 = 2 * math.pi * (np.outer(k2, m) % local) / local
     second = np.concatenate([np.cos(ang2), np.sin(ang2)], axis=1) / math.sqrt(length * GS)
     parts = []
@@ -394,45 +395,48 @@
                 at = pl.ds((2 * p + w) * rows, rows)
                 gp[at, lanes] = (re * cos + im * sin).astype(BF16)
                 gp[at, rest] = (im * cos - re * sin).astype(BF16)
-    spec = dot_nt(tab[:local], gp[...])
-    if rows == GS and lane == 128:
-        left = lax.broadcasted_iota(jnp.int32, (rows, lane), 1) < rows
-        for l in range(z.tiles):
-            for p in range(z.pairs):
-                t0 = spec[2 * l * rows:(2 * l + 1) * rows, p * lane:(p + 1) * lane]
-                t1 = spec[(2 * l + 1) * rows:(2 * l + 2) * rows, p * lane:(p + 1) * lane]
-                stage[l, pl.ds(2 * p, rows, stride=z.per), :] = jnp.where(
-                    left, t0, pltpu.roll(t1, rows, 1)
-                )
-                stage[l, pl.ds(2 * p + 1, rows, stride=z.per), :] = jnp.where(
-                    left, pltpu.roll(t0, rows, 1), t1
-                )
-    else:
-        full = spec.reshape(z.hops, rows, z.per, rows).transpose(1, 2, 0, 3)
-        full = full.reshape(rows * z.per, z.tiles, lane)
-        for l in range(z.tiles):
-            stage[l] = full[:, l]
-    for l in range(z.tiles):
-        back[:, :, l * lane:(l + 1) * lane] = stage[l].reshape(rows, z.per, lane).astype(BF16)
-
     pl.semaphore_wait(plane_sem, 1)
     seq = r // groups
     slot = h * groups + lax.rem(r, groups)
     target = 2 * x + seq
-
-    for k in range(nz):
-        pz = k // 2 + (k % 2) * (nz // 2)
-
-        def give(i, carry, pz=pz):
-            peer = pz * ny + lax.rem(yy + i, ny)
-            send(back.at[peer], got2.at[slot], b_send, b_recv, peer, target)
-            return carry
-
-        lax.fori_loop(1, ny, give, 0)
-
-        @pl.when(pz != zz)
-        def _(pz=pz, give=give):
-            give(0, 0)
+    hr = rows // 2
+    for half in range(2):
+        spec = dot_nt(tab[half * (local // 2):(half + 1) * (local // 2)], gp[...])
+        if rows == GS and lane == 128:
+            left = lax.broadcasted_iota(jnp.int32, (hr, lane), 1) < rows
+            for l in range(z.tiles):
+                for p in range(z.pairs):
+                    t0 = spec[2 * l * hr:(2 * l + 1) * hr, p * lane:(p + 1) * lane]
+                    t1 = spec[(2 * l + 1) * hr:(2 * l + 2) * hr, p * lane:(p + 1) * lane]
+                    at = half * hr * z.per + 2 * p
+                    stage[l, pl.ds(at, hr, stride=z.per), :] = jnp.where(
+                        left, t0, pltpu.roll(t1, rows, 1)
+                    )
+                    stage[l, pl.ds(at + 1, hr, stride=z.per), :] = jnp.where(
+                        left, pltpu.roll(t0, rows, 1), t1
+                    )
+        else:
+            full = spec.reshape(z.hops, hr, z.per, rows).transpose(1, 2, 0, 3)
+            full = full.reshape(hr * z.per, z.tiles, lane)
+            for l in range(z.tiles):
+                stage[l, half * hr * z.per:(half + 1) * hr * z.per] = full[:, l]
+        for l in range(z.tiles):
+            part = stage[l, half * hr * z.per:(half + 1) * hr * z.per]
+            back[half * hr:(half + 1) * hr, :, l * lane:(l + 1) * lane] = part.reshape(
+                hr, z.per, lane
+            ).astype(BF16)
+        for pz in range(half * (nz // 2), (half + 1) * (nz // 2)):
+
+            def give(i, carry, pz=pz):
+                peer = pz * ny + lax.rem(yy + i, ny)
+                send(back.at[peer], got2.at[slot], b_send, b_recv, peer, target)
+                return carry
+
+            lax.fori_loop(1, ny, give, 0)
+
+            @pl.when(pz != zz)
+            def _(give=give):
+                give(0, 0)
 
     @pl.when(seq == h)
     def _():

time: 58.4 us -> 58.9 us (level)
  no operation moved by 1% of the time
where the time goes in v6:
time: 58.9 us; the launch traced here: 58.7 us
  Pallas kernels  57.6 us (98%)
  local copies, waits for them, and re-layouts  1.15 us (2%)
    pallas_call x1, Pallas kernels, body(): pl.pallas_call(functools.partial(kernel, z), out_shape=jax.ShapeDtypeStru...  57.6 us

profile of v6, /device:TPU:1, one launch (start us, length us, event | category | flops | bytes accessed | tf_op | source)
XLA Modules:
  0.0 58.7 jit_solution(17738920278432906982)
XLA Ops:
  0.0 57.6 %fourier_mix.1 = bf16[384,2048]{1,0:T(8,128)(2,1)S(1)} custom-call(bf16[384,2048]{1,0:T(8,128)(2,1)} %bitcast.4, bf16[2048]{0:T(1024)(128)(2,1)} %gain_hbm.1, bf16[32,64]{1,0:T(8,128)(2,1)} %wi_hbm.1, bf16[32,64]{1,0:T(8,128)(2,1)} %bitcast.5, bf16[1280,768]{1,0:T(8,128)(2,1)} %constant.2.clone.tab_hbm), custom_call_target="tpu_custom_call" | custom-call | tf_op jit(solution)/shard_map/fourier_mix/pallas_call | solution.py:541
  57.6 1.1 %copy.7 = bf16[1,384,2048]{2,1,0:T(8,128)(2,1)} copy(bf16[1,384,2048]{2,1,0:T(8,128)(2,1)S(1)} %bitcast.3) | data formatting | bytes 3145728
